TPU v7x, 32 devices: a whole 2x2x4 slice. The times are simulated.
32 devices in a mesh: sp: 4 (over y, x), tp: 8 (over z, core).
Axes of the slice: x: 2, y: 2, z: 4, core: 2. Of those that a mesh axis runs over, the one named last changes fastest.
Arguments:
- tokens: bfloat16 [8192, 2048], P('sp', 'tp'), may hold values from -6 to 6
- norm_gain: float32 [2048], replicated, may hold values from 0.1 to 1.9
- w_key: bfloat16 [2048, 1024], P(None, 'tp'), may hold values from -0.125 to 0.125
- w_decay: bfloat16 [2048, 1024], P(None, 'tp'), may hold values from -0.125 to 0.125
- w_value: bfloat16 [2048, 512], replicated, may hold values from -0.125 to 0.125
- decay_bias: float32 [1024], P('tp'), may hold values from 0 to 8.5
- gate_drift: float32 [8192], P('sp'), may hold values from -1 to 1
- queries: bfloat16 [1024], P('tp'), may hold values from -6 to 6
- out_gain: float32 [4, 512], P(None, 'sp'), may hold values from 0.1 to 1.9
Outputs:
- state_cache: bfloat16 [1024, 512], P('tp', 'sp')
- first_read: float32 [4, 512], P(None, 'sp')
All inputs are finite; a program needn't handle non-finite values.
Results may differ from a plain program's by a relative error of at most 0.009.
Values may be sent and summed in bfloat16 or wider, within the bound.
A program may use at most 128 MiB of HBM per device.

v0:
```python
import jax
import jax.numpy as jnp
from jax import lax
from jax.sharding import PartitionSpec as P

QUERY_KEY_HEADS = 4
KEY_CHANNELS = 256
VALUE_CHANNELS = 512
EPS = 1e-06
GATE_NORM = 16.0


def body(tokens, norm_gain, w_key, w_decay, w_value, decay_bias, gate_drift, queries, out_gain):
    gathered = lax.all_gather(tokens, "tp", axis=1, tiled=True)
    rows_f32 = gathered.astype(jnp.float32)
    inverse_rms = lax.rsqrt(jnp.mean(rows_f32 * rows_f32, axis=1, keepdims=True) + EPS)
    normed = (rows_f32 * inverse_rms * norm_gain[None, :]).astype(jnp.bfloat16)
    key_proj = jnp.dot(normed, w_key, preferred_element_type=jnp.float32).astype(jnp.bfloat16)
    gate_pre = jnp.dot(normed, w_decay, preferred_element_type=jnp.float32).astype(jnp.bfloat16)
    value_proj = jnp.dot(normed, w_value, preferred_element_type=jnp.float32).astype(jnp.bfloat16)
    log_decay = (
        jax.nn.log_sigmoid(gate_pre.astype(jnp.float32) + decay_bias[None, :] + gate_drift[:, None])
        / GATE_NORM
    )
    suffix = lax.cumsum(log_decay, axis=0, reverse=True)
    weighted = (key_proj.astype(jnp.float32) * jnp.exp(suffix - log_decay)).astype(jnp.bfloat16)
    partial_value = lax.dot_general(
        weighted, value_proj, (((0,), (0,)), ((), ())), preferred_element_type=jnp.float32
    )
    total_decay = suffix[0]
    channels = partial_value.shape[0]
    span_count = lax.axis_size("sp")
    spread = jnp.broadcast_to(total_decay[None, :, None], (1, channels, span_count))
    blocks, totals = (
        lax.all_to_all(partial_value[None], "sp", split_axis=2, concat_axis=0, tiled=True),
        lax.all_to_all(spread, "sp", split_axis=2, concat_axis=0, tiled=True),
    )
    later_sum = lax.cumsum(totals, axis=0, reverse=True) - totals
    matrix_state = jnp.sum(jnp.exp(later_sum) * blocks, axis=0)
    state_cache = matrix_state.astype(jnp.bfloat16)
    channel_ids = lax.axis_index("tp") * channels + jnp.arange(channels, dtype=jnp.int32)
    owners = (channel_ids // KEY_CHANNELS)[:, None] == jnp.arange(QUERY_KEY_HEADS, dtype=jnp.int32)[
        None, :
    ]
    query_of_head = jnp.where(
        owners, queries.astype(jnp.float32)[:, None] * KEY_CHANNELS ** (-0.5), 0.0
    )
    part_read = lax.dot_general(
        query_of_head, matrix_state, (((0,), (0,)), ((), ())), precision=lax.Precision.HIGHEST
    )
    summed_read = lax.psum(part_read, "tp")
    squares = lax.psum(jnp.sum(summed_read * summed_read, axis=1), "sp")
    first_read = summed_read * lax.rsqrt(squares / VALUE_CHANNELS + EPS)[:, None] * out_gain
    return (state_cache, first_read)


def solution(mesh):
    return jax.shard_map(
        body,
        mesh=mesh,
        in_specs=(
            P("sp", "tp"),
            P(),
            P(None, "tp"),
            P(None, "tp"),
            P(),
            P("tp"),
            P("sp"),
            P("tp"),
            P(None, "sp"),
        ),
        out_specs=(P("tp", "sp"), P(None, "sp")),
        check_vma=False,
    )
```

profile of v0, /device:TPU:0, one launch (start us, length us, event | category | flops | bytes accessed | tf_op | source)
XLA Modules:
  0.0 171.0 jit_solution(2722808447826279931)
XLA Ops:
  7.2 0.0 copy-start
  7.2 0.0 copy-start.5
  7.2 0.0 copy-start.3
  7.2 0.0 copy-start.6
  7.2 0.0 copy-start.4
  7.2 0.0 all-gather.2.cloned.1.call-start
  7.3 0.7 all-gather.2.cloned.1.call-update
  8.0 0.7 convert_multiply_fusion.2
  8.7 86.2 %all-gather.2.cloned.1.call-done = bf16[2048,2048]{1,0:T(8,128)(2,1)} async-done(((bf16[2048,256]{1,0:T(8,128)(2,1)}), bf16[2048,2048]{1,0:T(8,128)(2,1)}) %all-gather.2.cloned.1.call-update) | async-done | bytes 8388624 | tf_op jit(solution)/shard_map/all_gather | solution.py:14
  94.9 5.2 %fusion = f32[2048]{0:T(1024)S(1)} fusion(bf16[2048,2048]{1,0:T(8,128)(2,1)} %all-gather.2.cloned.1.call-done), kind=kLoop, calls=%fused_computation.2 | loop fusion | flops 12580864 | bytes 8396800 | tf_op jit(solution)/shard_map/reduce_sum | solution.py:16
  100.1 0.0 copy-done.5
  100.1 0.0 copy-done.3
  100.1 0.0 copy-done.6
  100.1 0.0 copy-done.4
  100.1 0.5 copy-done.1
  100.6 4.7 %fusion.12 = (f32[128,2048]{0,1:T(8,128)S(1)}, f32[2048,128]{1,0:T(8,128)}) fusion(f32[2048]{0:T(1024)S(1)} %copy-done.4, f32[128]{0:T(128)S(1)} %copy-done.6, bf16[2048,128]{1,0:T(8,128)(2,1)S(1)} %copy-done.3, bf16[2048,2048]{1,0:T(8,128)(2,1)S(1)} %copy-done.1, f32[2048]{0:T(1024)S(1)} %copy-done.5, f32[2048]{0:T(1024)S(1)} %add_rsqrt_fusion), kind=kOutput, calls=%fused_computation.19 | convolution fusion | flops 1093926912 | bytes 11035136 | tf_op jit(solution)/shard_map/dot_general | solution.py:19
  105.4 2.6 %fusion.21 = f32[128,16,128]{0,1,2:T(8,128)S(1)} fusion(f32[128,16,128]{0,2,1:T(8,128)S(1)} %bitcast.44), kind=kOutput, calls=%fused_computation.30 | output fusion | flops 33292288 | bytes 2097152 | tf_op jit(solution)/shard_map/reduce-window
  108.0 0.1 broadcast_add_fusion
  108.1 0.3 copy.17
  108.4 0.6 broadcast_in_dim.19
  109.0 3.6 %all-to-all-start = ((f32[1,128,4]{1,0,2:T(1,128)}), f32[1,128,4]{1,0,2:T(1,128)S(1)}, u32[]{:S(2)}, u32[]{:S(2)}) async-start(f32[1,128,4]{1,0,2:T(1,128)} %broadcast_in_dim.19), calls=%async_computation | async-start | bytes 4096 | tf_op jit(solution)/shard_map/all_to_all | solution.py:36
  112.6 7.6 %fusion.9 = bf16[2048,128]{1,0:T(8,128)(2,1)} fusion(bf16[2048,128]{1,0:T(8,128)(2,1)} %param.11, f32[2048,128]{1,0:T(8,128)S(1)} %bitcast.43, f32[2048,128]{1,0:T(8,128)} %get-tuple-element.5, bf16[2048,2048]{1,0:T(8,128)(2,1)} %all-gather.2.cloned.1.call-done, f32[2048]{0:T(1024)S(1)} %copy-done.5, f32[2048]{0:T(1024)S(1)} %add_rsqrt_fusion), kind=kOutput, calls=%fused_computation.16 | convolution fusion | flops 1093926912 | bytes 11550720 | tf_op jit(solution)/shard_map/dot_general | solution.py:18
  120.2 10.2 %fusion.10 = f32[128,512]{0,1:T(8,128)} fusion(bf16[2048,128]{1,0:T(8,128)(2,1)} %fusion.9, bf16[2048,512]{1,0:T(8,128)(2,1)S(1)} %copy-done, bf16[2048,2048]{1,0:T(8,128)(2,1)} %all-gather.2.cloned.1.call-done, f32[2048]{0:T(1024)S(1)} %copy-done.5, f32[2048]{0:T(1024)S(1)} %add_rsqrt_fusion), kind=kOutput, calls=%fused_computation.17 | convolution fusion | flops 4581228544 | bytes 11288576 | tf_op jit(solution)/shard_map/dot_general | solution.py:27
  130.4 0.0 all-to-all-done
  130.5 4.2 %all-to-all-start.1 = ((f32[1,128,512]{1,0,2:T(1,128)}), f32[1,128,512]{1,0,2:T(1,128)S(1)}, u32[]{:S(2)}, u32[]{:S(2)}) async-start(f32[1,128,512]{1,0,2:T(1,128)} %bitcast.18), calls=%async_computation.1 | async-start | bytes 524288 | tf_op jit(solution)/shard_map/all_to_all | solution.py:35
  134.7 5.3 %all-to-all-done.1 = f32[1,128,512]{1,0,2:T(1,128)S(1)} async-done(((f32[1,128,512]{1,0,2:T(1,128)}), f32[1,128,512]{1,0,2:T(1,128)S(1)}, u32[]{:S(2)}, u32[]{:S(2)}) %all-to-all-start.1) | async-done | bytes 262176 | tf_op jit(solution)/shard_map/all_to_all | solution.py:35
  140.0 0.3 fusion.23
  140.3 13.6 %psum.14 = f32[4,128]{1,0:T(4,128)S(1)} all-reduce(f32[4,128]{1,0:T(4,128)S(1)} %fusion.23), channel_id=1, replica_groups=mesh['sp'=4,'tp'=8] {'tp'}, use_global_device_ids=true, to_apply=%region_5.6 | all-reduce | flops 512 | bytes 4096 | tf_op jit(solution)/shard_map/psum | solution.py:51
  153.9 0.1 multiply_reduce_fusion.1
  154.1 8.7 %psum.15 = f32[4]{0:T(128)S(1)} all-reduce(f32[4]{0:T(128)S(1)} %multiply_reduce_fusion.1), channel_id=1, replica_groups=mesh['sp'=4,'tp'=8] {'sp'}, use_global_device_ids=true, to_apply=%region_7.8 | all-reduce | flops 4 | bytes 32 | tf_op jit(solution)/shard_map/psum | solution.py:52
  162.8 0.7 copy.19
  163.5 0.6 multiply_multiply_fusion
  (15 shorter events, 0.2 us)
Async XLA Ops:
  7.2 113.1 %copy-start = (bf16[2048,512]{1,0:T(8,128)(2,1)S(1)}, bf16[2048,512]{1,0:T(8,128)(2,1)}, u32[]{:S(2)}) copy-start(bf16[2048,512]{1,0:T(8,128)(2,1)} %param.13) | copy-start | bytes 6291460
  7.2 92.9 %copy-start.5 = (f32[2048]{0:T(1024)S(1)}, f32[2048]{0:T(1024)}, u32[]{:S(2)}) copy-start(f32[2048]{0:T(1024)} %param.10) | copy-start | bytes 24580
  7.2 92.9 %copy-start.3 = (bf16[2048,128]{1,0:T(8,128)(2,1)S(1)}, bf16[2048,128]{1,0:T(8,128)(2,1)}, u32[]{:S(2)}) copy-start(bf16[2048,128]{1,0:T(8,128)(2,1)} %param.12) | copy-start | bytes 1572868
  7.2 92.9 %copy-start.6 = (f32[128]{0:T(128)S(1)}, f32[128]{0:T(128)}, u32[]{:S(2)}) copy-start(f32[128]{0:T(128)} %param.14) | copy-start | bytes 1540
  7.2 92.9 %copy-start.4 = (f32[2048]{0:T(1024)S(1)}, f32[2048]{0:T(1024)}, u32[]{:S(2)}) copy-start(f32[2048]{0:T(1024)} %param.15) | copy-start | bytes 24580
  7.2 87.6 %all-gather.2.cloned.1.call-start = ((), (), s32[]{:S(2)}) async-start(), calls=%async_computation.2 | async-start | bytes 9437184 | tf_op jit(solution)/shard_map/all_gather | solution.py:14
  94.9 5.8 %copy-start.1 = (bf16[2048,2048]{1,0:T(8,128)(2,1)S(1)}, bf16[2048,2048]{1,0:T(8,128)(2,1)}, u32[]{:S(2)}) copy-start(bf16[2048,2048]{1,0:T(8,128)(2,1)} %all-gather.2.cloned.1.call-done) | copy-start | bytes 25165828
  109.0 21.5 %all-to-all-start = ((f32[1,128,4]{1,0,2:T(1,128)}), f32[1,128,4]{1,0,2:T(1,128)S(1)}, u32[]{:S(2)}, u32[]{:S(2)}) async-start(f32[1,128,4]{1,0,2:T(1,128)} %broadcast_in_dim.19), calls=%async_computation | async-start | bytes 4096 | tf_op jit(solution)/shard_map/all_to_all | solution.py:36
  120.2 43.3 %copy-start.2 = (f32[4,128]{1,0:T(4,128)S(1)}, f32[4,128]{1,0:T(4,128)}, u32[]{:S(2)}) copy-start(f32[4,128]{1,0:T(4,128)} %param.17) | copy-start | bytes 6148
  130.5 9.6 %all-to-all-start.1 = ((f32[1,128,512]{1,0,2:T(1,128)}), f32[1,128,512]{1,0,2:T(1,128)S(1)}, u32[]{:S(2)}, u32[]{:S(2)}) async-start(f32[1,128,512]{1,0,2:T(1,128)} %bitcast.18), calls=%async_computation.1 | async-start | bytes 524288 | tf_op jit(solution)/shard_map/all_to_all | solution.py:35
Sparse Core Ops, SparseCore 0:
  9.6 85.1 all-gather.1
where the time goes:
time: 171 us
  waiting for transfers between devices  92.2 us (54%)
  matrix products  22.8 us (13%)
  blocking collectives  22.4 us (13%)
  between operations  14.2 us (8%)
  other arithmetic  9.45 us (6%)
  starting transfers between devices  7.88 us (5%)
  local copies, waits for them, and re-layouts  2.17 us (1%)
    all_gather x1, waiting for transfers between devices, body(): gathered = lax.all_gather(tokens, 'tp', axis=1, tiled=True)  86.2 us
    psum x1, blocking collectives, body(): summed_read = lax.psum(part_read, 'tp')  13.6 us
    dot_general x1, matrix products, body(): lax.dot_general(weighted, value_proj, (((0,), (0,)), ((), ())), preferred...  10.2 us
    psum x1, blocking collectives, body(): squares = lax.psum(jnp.sum(summed_read * summed_read, axis=1), 'sp')  8.74 us
    dot_general x1, matrix products, body(): jnp.dot(normed, w_key, preferred_element_type=jnp.float32)  7.58 us
    all_to_all x1, waiting for transfers between devices, body(): lax.all_to_all(partial_value[None], 'sp', split_axis=2, concat_axis=0, ti...  5.33 us
    reduce_sum x1, other arithmetic, body(): jnp.mean(rows_f32 * rows_f32, axis=1, keepdims=True) + EPS  5.23 us
    dot_general x1, matrix products, body(): jnp.dot(normed, w_decay, preferred_element_type=jnp.float32)  4.74 us
  transfers between devices with their start and end apart: 3, of which 2 were waited for; matrix products, arithmetic and copies ran while one was open for 11% of the time, Pallas kernels for 0%

commit v1 on v0

--- a/solution.py
+++ b/solution.py
@@ -11,7 +11,9 @@
 
 
 def body(tokens, norm_gain, w_key, w_decay, w_value, decay_bias, gate_drift, queries, out_gain):
-    gathered = lax.all_gather(tokens, "tp", axis=1, tiled=True)
+    gathered = jnp.concatenate(
+        lax.all_to_all(jnp.stack([tokens] * lax.axis_size("tp")), "tp", 0, 0), axis=1
+    )
     rows_f32 = gathered.astype(jnp.float32)
     inverse_rms = lax.rsqrt(jnp.mean(rows_f32 * rows_f32, axis=1, keepdims=True) + EPS)
     normed = (rows_f32 * inverse_rms * norm_gain[None, :]).astype(jnp.bfloat16)

time: 171 us -> 277 us (1.62)
  waiting for transfers between devices: 92.2 us -> 189 us
  between operations: 14.2 us -> 0.77 us
  other arithmetic: 9.45 us -> 17.2 us
  starting transfers between devices: 7.88 us -> 14.5 us
  local copies, waits for them, and re-layouts: 2.17 us -> 7.62 us
    all_to_all x0 -> x1, waiting for transfers between devices: none -> 184 us  [body(): lax.all_to_all(jnp.stack([tokens] * lax.axis_size('tp')), 'tp', 0, 0)]
    all_gather x1 -> x0, waiting for transfers between devices: 86.2 us -> none  [body(): gathered = lax.all_gather(tokens, 'tp', axis=1, tiled=True)]
    convert_element_type x0 -> x1, other arithmetic: none -> 8.58 us  [body(): normed = (rows_f32 * inverse_rms * norm_gain[None, :]).astype(jnp.bfloat16)]
    all_to_all x0 -> x1, starting transfers between devices: none -> 6.49 us  [body(): lax.all_to_all(jnp.stack([tokens] * lax.axis_size('tp')), 'tp', 0, 0)]
    another operation x2 -> x3, local copies, waits for them, and re-layouts: 0.01 us -> 4.29 us  [the longest x1 4.28 us: body(): jnp.stack([tokens] * lax.axis_size('tp'))]
    dot_general x1, matrix products: 4.74 us -> 7.51 us  [body(): jnp.dot(normed, w_decay, preferred_element_type=jnp.float32)]
  transfers between devices with their start and end apart: 3 -> 3, of which waited for: 2 -> 2; matrix products, arithmetic and copies ran while one was open for 11% -> 6% of each run, Pallas kernels for 0% -> 0%
where the time goes in v1:
time: 277 us
  waiting for transfers between devices  189 us (68%)
  matrix products  25.3 us (9%)
  blocking collectives  22.4 us (8%)
  other arithmetic  17.2 us (6%)
  starting transfers between devices  14.5 us (5%)
  local copies, waits for them, and re-layouts  7.62 us (3%)
    all_to_all x1, waiting for transfers between devices, body(): lax.all_to_all(jnp.stack([tokens] * lax.axis_size('tp')), 'tp', 0, 0)  184 us
    psum x1, blocking collectives, body(): summed_read = lax.psum(part_read, 'tp')  13.6 us
    dot_general x1, matrix products, body(): lax.dot_general(weighted, value_proj, (((0,), (0,)), ((), ())), preferred...  10.1 us
    psum x1, blocking collectives, body(): squares = lax.psum(jnp.sum(summed_read * summed_read, axis=1), 'sp')  8.74 us
    convert_element_type x1, other arithmetic, body(): normed = (rows_f32 * inverse_rms * norm_gain[None, :]).astype(jnp.bfloat16)  8.58 us
    dot_general x1, matrix products, body(): jnp.dot(normed, w_decay, preferred_element_type=jnp.float32)  7.51 us
    dot_general x1, matrix products, body(): jnp.dot(normed, w_key, preferred_element_type=jnp.float32)  7.37 us
    all_to_all x1, starting transfers between devices, body(): lax.all_to_all(jnp.stack([tokens] * lax.axis_size('tp')), 'tp', 0, 0)  6.49 us
  transfers between devices with their start and end apart: 3, of which 2 were waited for; matrix products, arithmetic and copies ran while one was open for 6% of the time, Pallas kernels for 0%

profile of v1, /device:TPU:0, one launch (start us, length us, event | category | flops | bytes accessed | tf_op | source)
XLA Modules:
  0.0 277.0 jit_solution(8849921225284389855)
XLA Ops:
  0.6 0.0 copy-start
  0.6 1.6 copy.20
  2.3 4.3 %stack.2 = bf16[8,2048,256]{1,2,0:T(8,128)(2,1)} broadcast(bf16[2048,256]{0,1:T(8,128)(2,1)S(1)} %copy.20), dimensions={1,2} | broadcast | bytes 9437184 | tf_op jit(solution)/shard_map/stack | solution.py:15
  6.6 6.5 %all-to-all-start = ((bf16[8,2048,256]{1,2,0:T(8,128)(2,1)}), bf16[8,2048,256]{1,2,0:T(8,128)(2,1)}, u32[]{:S(2)}, u32[]{:S(2)}) async-start(bf16[8,2048,256]{1,2,0:T(8,128)(2,1)} %stack.2), calls=%async_computation | async-start | bytes 16777216 | tf_op jit(solution)/shard_map/all_to_all | solution.py:15
  13.1 0.0 copy-done.5
  13.1 183.9 %all-to-all-done = bf16[8,2048,256]{1,2,0:T(8,128)(2,1)} async-done(((bf16[8,2048,256]{1,2,0:T(8,128)(2,1)}), bf16[8,2048,256]{1,2,0:T(8,128)(2,1)}, u32[]{:S(2)}, u32[]{:S(2)}) %all-to-all-start) | async-done | bytes 8388640 | tf_op jit(solution)/shard_map/all_to_all | solution.py:15
  197.0 5.1 %multiply_reduce_fusion = f32[2048]{0:T(1024)S(1)} fusion(bf16[8,2048,256]{1,2,0:T(8,128)(2,1)} %all-to-all-done), kind=kLoop, calls=%fused_computation.3 | loop fusion | flops 12580864 | bytes 8396800 | tf_op jit(solution)/shard_map/reduce_sum | solution.py:18
  202.1 0.0 copy-done.1
  202.2 0.0 copy-start.3
  202.2 0.0 copy-start.4
  202.2 0.0 copy-start.6
  202.2 8.6 %fusion.1 = bf16[2048,2048]{0,1:T(8,128)(2,1)} fusion(f32[2048]{0:T(1024)S(1)} %copy-done.1, f32[2048]{0:T(1024)S(1)} %add_rsqrt_fusion, bf16[8,2048,256]{1,2,0:T(8,128)(2,1)} %all-to-all-done), kind=kLoop, calls=%fused_computation.2 | loop fusion | flops 16777216 | bytes 16793600 | tf_op jit(solution)/shard_map/convert_element_type | solution.py:19
  210.8 0.0 copy-done.3
  210.8 0.0 copy-done.4
  210.8 0.0 copy-done.6
  210.8 7.5 %fusion.11 = (f32[128,2048]{0,1:T(8,128)S(1)}, f32[2048,128]{1,0:T(8,128)}) fusion(f32[2048]{0:T(1024)S(1)} %copy-done.4, f32[128]{0:T(128)S(1)} %copy-done.6, bf16[2048,2048]{0,1:T(8,128)(2,1)} %fusion.1, bf16[2048,128]{1,0:T(8,128)(2,1)S(1)} %copy-done.3), kind=kOutput, calls=%fused_computation.18 | convolution fusion | flops 1077149696 | bytes 11018752 | tf_op jit(solution)/shard_map/dot_general | solution.py:21
  218.3 2.6 fusion.20
  220.9 0.1 broadcast_add_fusion
  221.0 0.3 copy.22
  221.4 0.6 broadcast_in_dim.19
  221.9 3.8 %all-to-all-start.1 = ((f32[1,128,4]{1,0,2:T(1,128)}), f32[1,128,4]{1,0,2:T(1,128)S(1)}, u32[]{:S(2)}, u32[]{:S(2)}) async-start(f32[1,128,4]{1,0,2:T(1,128)} %broadcast_in_dim.19), calls=%async_computation.1 | async-start | bytes 4096 | tf_op jit(solution)/shard_map/all_to_all | solution.py:38
  225.7 7.4 %fusion.8 = bf16[2048,128]{1,0:T(8,128)(2,1)} fusion(bf16[2048,2048]{0,1:T(8,128)(2,1)} %fusion.1, bf16[2048,128]{1,0:T(8,128)(2,1)} %param.11, f32[2048,128]{1,0:T(8,128)S(1)} %bitcast.54, f32[2048,128]{1,0:T(8,128)} %get-tuple-element.5), kind=kOutput, calls=%fused_computation.15 | convolution fusion | flops 1077149696 | bytes 11534336 | tf_op jit(solution)/shard_map/dot_general | solution.py:20
  233.1 10.1 %fusion.9 = f32[128,512]{0,1:T(8,128)} fusion(bf16[2048,128]{1,0:T(8,128)(2,1)} %fusion.8, bf16[2048,2048]{0,1:T(8,128)(2,1)} %fusion.1, bf16[2048,512]{1,0:T(8,128)(2,1)S(1)} %copy-done), kind=kOutput, calls=%fused_computation.16 | convolution fusion | flops 4564451328 | bytes 11272192 | tf_op jit(solution)/shard_map/dot_general | solution.py:29
  243.2 0.0 all-to-all-done.1
  243.2 4.2 %all-to-all-start.2 = ((f32[1,128,512]{1,0,2:T(1,128)}), f32[1,128,512]{1,0,2:T(1,128)S(1)}, u32[]{:S(2)}, u32[]{:S(2)}) async-start(f32[1,128,512]{1,0,2:T(1,128)} %bitcast.21), calls=%async_computation.2 | async-start | bytes 524288 | tf_op jit(solution)/shard_map/all_to_all | solution.py:37
  247.5 5.3 %all-to-all-done.2 = f32[1,128,512]{1,0,2:T(1,128)S(1)} async-done(((f32[1,128,512]{1,0,2:T(1,128)}), f32[1,128,512]{1,0,2:T(1,128)S(1)}, u32[]{:S(2)}, u32[]{:S(2)}) %all-to-all-start.2) | async-done | bytes 262176 | tf_op jit(solution)/shard_map/all_to_all | solution.py:37
  252.8 0.3 fusion.22
  253.1 13.6 %psum.14 = f32[4,128]{1,0:T(4,128)S(1)} all-reduce(f32[4,128]{1,0:T(4,128)S(1)} %fusion.22), channel_id=1, replica_groups=mesh['sp'=4,'tp'=8] {'tp'}, use_global_device_ids=true, to_apply=%region_5.6 | all-reduce | flops 512 | bytes 4096 | tf_op jit(solution)/shard_map/psum | solution.py:53
  266.7 0.1 multiply_reduce_fusion.2
  266.8 8.7 %psum.15 = f32[4]{0:T(128)S(1)} all-reduce(f32[4]{0:T(128)S(1)} %multiply_reduce_fusion.2), channel_id=1, replica_groups=mesh['sp'=4,'tp'=8] {'sp'}, use_global_device_ids=true, to_apply=%region_7.8 | all-reduce | flops 4 | bytes 32 | tf_op jit(solution)/shard_map/psum | solution.py:54
  275.6 0.7 copy.24
  276.3 0.6 multiply_multiply_fusion
  (17 shorter events, 0.2 us)
Async XLA Ops:
  0.6 232.5 %copy-start = (bf16[2048,512]{1,0:T(8,128)(2,1)S(1)}, bf16[2048,512]{1,0:T(8,128)(2,1)}, u32[]{:S(2)}) copy-start(bf16[2048,512]{1,0:T(8,128)(2,1)} %param.13) | copy-start | bytes 6291460
  6.6 6.5 %copy-start.5 = (bf16[128]{0:T(256)(128)(2,1)S(1)}, bf16[128]{0:T(256)(128)(2,1)}, u32[]{:S(2)}) copy-start(bf16[128]{0:T(256)(128)(2,1)} %param.16) | copy-start | bytes 772
  6.6 190.4 %all-to-all-start = ((bf16[8,2048,256]{1,2,0:T(8,128)(2,1)}), bf16[8,2048,256]{1,2,0:T(8,128)(2,1)}, u32[]{:S(2)}, u32[]{:S(2)}) async-start(bf16[8,2048,256]{1,2,0:T(8,128)(2,1)} %stack.2), calls=%async_computation | async-start | bytes 16777216 | tf_op jit(solution)/shard_map/all_to_all | solution.py:15
  13.1 189.1 %copy-start.1 = (f32[2048]{0:T(1024)S(1)}, f32[2048]{0:T(1024)}, u32[]{:S(2)}) copy-start(f32[2048]{0:T(1024)} %param.10) | copy-start | bytes 24580
  202.2 8.6 %copy-start.3 = (bf16[2048,128]{1,0:T(8,128)(2,1)S(1)}, bf16[2048,128]{1,0:T(8,128)(2,1)}, u32[]{:S(2)}) copy-start(bf16[2048,128]{1,0:T(8,128)(2,1)} %param.12) | copy-start | bytes 1572868
  202.2 8.6 %copy-start.4 = (f32[2048]{0:T(1024)S(1)}, f32[2048]{0:T(1024)}, u32[]{:S(2)}) copy-start(f32[2048]{0:T(1024)} %param.15) | copy-start | bytes 24580
  202.2 8.6 %copy-start.6 = (f32[128]{0:T(128)S(1)}, f32[128]{0:T(128)}, u32[]{:S(2)}) copy-start(f32[128]{0:T(128)} %param.14) | copy-start | bytes 1540
  221.9 21.3 %all-to-all-start.1 = ((f32[1,128,4]{1,0,2:T(1,128)}), f32[1,128,4]{1,0,2:T(1,128)S(1)}, u32[]{:S(2)}, u32[]{:S(2)}) async-start(f32[1,128,4]{1,0,2:T(1,128)} %broadcast_in_dim.19), calls=%async_computation.1 | async-start | bytes 4096 | tf_op jit(solution)/shard_map/all_to_all | solution.py:38
  233.1 43.2 %copy-start.2 = (f32[4,128]{1,0:T(4,128)S(1)}, f32[4,128]{1,0:T(4,128)}, u32[]{:S(2)}) copy-start(f32[4,128]{1,0:T(4,128)} %param.17) | copy-start | bytes 6148
  243.2 9.6 %all-to-all-start.2 = ((f32[1,128,512]{1,0,2:T(1,128)}), f32[1,128,512]{1,0,2:T(1,128)S(1)}, u32[]{:S(2)}, u32[]{:S(2)}) async-start(f32[1,128,512]{1,0,2:T(1,128)} %bitcast.21), calls=%async_computation.2 | async-start | bytes 524288 | tf_op jit(solution)/shard_map/all_to_all | solution.py:37
